TPU v7x, 512 devices: a whole 4x8x8 slice. The times are simulated.
512 devices in a mesh: sp: 64 (over z, y), tp: 8 (over x, core).
Axes of the slice: x: 4, y: 8, z: 8, core: 2. Of those that a mesh axis runs over, the one named last changes fastest.
Arguments:
- inputs: bfloat16 [24576, 2048], P(('sp', 'tp')), may hold values from -6 to 6
- norm_gain: float32 [2048], replicated, may hold values from 0.1 to 1.9
- latent_down: bfloat16 [2048, 256], P('sp'), may hold values from -0.125 to 0.125
- rope_down: bfloat16 [2048, 64], P('sp'), may hold values from -0.125 to 0.125
- latent_gain: float32 [256], replicated, may hold values from 0.1 to 1.9
- mla_query: bfloat16 [2048, 1536], P(None, 'tp'), as said below
- key_up: bfloat16 [256, 1024], replicated, may hold values from -3.5 to 3.5
- value_up: bfloat16 [256, 1024], replicated, may hold values from -1.75 to 1.75
- swa_query: bfloat16 [2048, 1024], P(None, 'tp'), as said below
- swa_key: bfloat16 [2048, 512], P(None, 'tp'), may hold values from -0.125 to 0.125
- swa_value: bfloat16 [2048, 512], P(None, 'tp'), may hold values from -0.125 to 0.125
- sink_logits: float32 [16], replicated, may hold values from 1 to 6
- out_mla: bfloat16 [1024, 2048], P(None, 'tp'), may hold values from -0.875 to 0.875
- out_swa: bfloat16 [1024, 2048], P(None, 'tp'), may hold values from -0.875 to 0.875
Outputs:
- mixed: bfloat16 [24576, 2048], P('sp', 'tp')
Inputs may be any that keep to these rules, and one draw needn't show every extreme that they name: `mla_query`: entries lie within 360 / sqrt(2048) in magnitude. `swa_query`: entries lie within 900 / sqrt(2048) in magnitude.
All inputs are finite; a program needn't handle non-finite values.
Results may differ from a plain program's by a relative error of at most 0.02.
The roundings to bfloat16 on the way count: a program that leaves them out, or rounds other values in their place, can miss the bound.
Values may be sent and summed in bfloat16 or wider, within the bound.
No kernel may reach another device: no remote copies, remote signals or barrier semaphores. Data moves between devices by JAX's collectives and lax.ppermute only.
A program may use at most 64 MiB of HBM per device.

v0:
```python
import math
import jax
import jax.numpy as jnp
from jax import lax
from jax.sharding import Mesh
from jax.sharding import PartitionSpec as P

NOPE = 128
ROPE = 64
VDIM = 128
KV_RANK = 256
HEAD = 64
WINDOW = 128
SP = ("sp_0", "sp_1")
SP_TP = ("sp_0", "sp_1", "tp")
NORM_EPS = 1e-06
ROPE_BASE = 10000.0
MASKED_VALUE = -1e30
KEY_SPAN = 512


def joined_along(tiles, dim):
    tiles = jnp.moveaxis(tiles, 0, dim)
    lengths = tiles.shape
    return tiles.reshape(*lengths[:dim], lengths[dim] * lengths[dim + 1], *lengths[dim + 2 :])


def copy_for_each(array, axis):
    copies = jnp.broadcast_to(array, (lax.axis_size(axis), *array.shape))
    return lax.all_to_all(copies, axis, split_axis=0, concat_axis=0, tiled=True)


def gathered_copies(array, axis, dim):
    return joined_along(copy_for_each(array, axis), dim)


def in_one_piece(arrays, axis, dim, along):
    ends, at = ([], 0)
    for a in arrays[:-1]:
        at += a.shape[along]
        ends.append(at)
    both = jnp.concatenate(arrays, axis=along)
    return tuple(jnp.split(lax.all_gather(both, axis, axis=dim, tiled=True), ends, axis=along))


def stacked_from(array, axes, turns):
    tiles = array[None]
    for k in turns:
        tiles = lax.all_gather(tiles, axes[k], axis=0, tiled=True)
    held = [lax.axis_size(axes[k]) for k in reversed(turns)]
    tiles = tiles.reshape(*held, *array.shape)
    turned = sorted(range(len(turns)), key=lambda place: turns[len(turns) - 1 - place])
    return tiles.transpose(*turned, *range(len(turns), tiles.ndim)).reshape(-1, *array.shape)


def gather_axes(array, axes, turns, dim):
    return joined_along(stacked_from(array, axes, turns), dim)


def of_everyone(array, axis):
    everything = copy_for_each(array, axis)
    return jnp.max(everything, axis=0)


def in_one_piece_2(arrays, axis, dim, along):
    widths = [math.prod(a.shape[along:]) for a in arrays]
    both = jnp.concatenate(
        [a.reshape(*a.shape[:along], w) for a, w in zip(arrays, widths)], axis=along
    )
    result = lax.psum_scatter(both, axis, scatter_dimension=dim, tiled=True)
    tiles = jnp.split(result, [sum(widths[:k]) for k in range(1, len(widths))], axis=along)
    return tuple(
        (b.reshape(*result.shape[:along], *a.shape[along:]) for a, b in zip(arrays, tiles))
    )


def from_behind(value, axis, steps):
    count = lax.axis_size(axis)
    first, last = (max(0, -steps), min(count, count - steps))
    return lax.ppermute(value, axis, [(source, source + steps) for source in range(first, last)])


def to_float(values):
    return lax.optimization_barrier(values).astype(jnp.float32)


def norm_rows(values, gains):
    widened = to_float(values)
    scaled = widened * lax.rsqrt(jnp.mean(widened * widened, axis=-1, keepdims=True) + NORM_EPS)
    return (scaled * gains).astype(jnp.bfloat16)


def rotate(values, positions):
    full_width = values.shape[-1]
    half_width = full_width // 2
    inverse = ROPE_BASE ** (-jnp.arange(0, full_width, 2, dtype=jnp.float32) / full_width)
    angles = positions.astype(jnp.float32)[:, None] * inverse[None, :]
    shaped = (values.shape[0],) + (1,) * (values.ndim - 2) + (half_width,)
    cos_table = jnp.cos(angles).reshape(shaped)
    sin_table = jnp.sin(angles).reshape(shaped)
    widened = to_float(values)
    first_half = widened[..., :half_width]
    second_half = widened[..., half_width:]
    return jnp.concatenate(
        [
            first_half * cos_table - second_half * sin_table,
            first_half * sin_table + second_half * cos_table,
        ],
        axis=-1,
    ).astype(jnp.bfloat16)


def attend_latent(
    state_in, keys_latent, keys_rope, key_positions, query_latent, query_rope, query_pos, mla_scale
):
    key_count = keys_latent.shape[0]
    span_rows = math.gcd(key_count, KEY_SPAN)
    last_query = query_pos[-1]

    def update(step_index, state):
        span_pos = lax.dynamic_slice_in_dim(key_positions, step_index * span_rows, span_rows, 0)

        def compute(current):
            running_max, denom_sum, weighted = current
            lat_block = lax.dynamic_slice_in_dim(keys_latent, step_index * span_rows, span_rows, 0)
            rope_block = lax.dynamic_slice_in_dim(keys_rope, step_index * span_rows, span_rows, 0)
            scores = (
                jnp.einsum(
                    "htj,sj->hts", query_latent, lat_block, preferred_element_type=jnp.float32
                )
                + jnp.einsum(
                    "htd,sd->hts", query_rope, rope_block, preferred_element_type=jnp.float32
                )
            ) * mla_scale
            allowed = span_pos[None, None, :] <= query_pos[None, :, None]
            scores = jnp.where(allowed, scores, MASKED_VALUE)
            new_max = jnp.maximum(running_max, jnp.max(scores, axis=-1))
            weights_raw = jnp.where(allowed, jnp.exp(scores - new_max[..., None]), 0.0)
            rescale = jnp.exp(running_max - new_max)
            denom_sum = denom_sum * rescale + jnp.sum(weights_raw, axis=-1)
            weighted = weighted * rescale[..., None] + jnp.einsum(
                "hts,sj->htj",
                weights_raw.astype(jnp.bfloat16),
                lat_block,
                preferred_element_type=jnp.float32,
            )
            return (new_max, denom_sum, weighted)

        return lax.cond(span_pos[0] <= last_query, compute, lambda current: current, state)

    return lax.fori_loop(0, key_count // span_rows, update, state_in)


def shards(
    inputs,
    norm_gain,
    latent_down,
    rope_down,
    latent_gain,
    mla_query,
    key_up,
    value_up,
    swa_query,
    swa_key,
    swa_value,
    sink_logits,
    out_mla,
    out_swa,
):
    own_rows = inputs.shape[0]
    tp_count = lax.axis_size("tp")
    block_rows = own_rows * tp_count
    tp_rank = lax.axis_index("tp")
    offset = lax.axis_index(SP) * block_rows
    own_pos = offset + tp_rank * own_rows + jnp.arange(own_rows, dtype=jnp.int32)
    block_pos = offset + jnp.arange(block_rows, dtype=jnp.int32)
    width_mla = mla_query.shape[1]
    width_swa = swa_query.shape[1]
    width_kv = swa_key.shape[1]
    heads_mla = width_mla // (NOPE + ROPE)
    heads_swa = width_swa // HEAD
    groups_kv = width_kv // HEAD
    group = heads_swa // groups_kv
    normed = norm_rows(inputs, norm_gain)
    pieces = gathered_copies(normed, "tp", 0)
    projected = jnp.concatenate(
        [
            jnp.dot(pieces, mla_query, preferred_element_type=jnp.float32).astype(jnp.bfloat16),
            jnp.dot(pieces, swa_query, preferred_element_type=jnp.float32).astype(jnp.bfloat16),
            jnp.dot(pieces, swa_key, preferred_element_type=jnp.float32).astype(jnp.bfloat16),
            jnp.dot(pieces, swa_value, preferred_element_type=jnp.float32).astype(jnp.bfloat16),
        ],
        axis=1,
    )
    pieces = in_one_piece((latent_down, rope_down), SP, 0, 1)
    latent = jnp.dot(normed, pieces[0], preferred_element_type=jnp.float32)
    rope_raw = jnp.dot(normed, pieces[1], preferred_element_type=jnp.float32)
    keys_latent = norm_rows(latent.astype(jnp.bfloat16), latent_gain)
    keys_rope = rotate(rope_raw.astype(jnp.bfloat16), own_pos)
    queries = projected[:, :width_mla].reshape(block_rows, heads_mla, NOPE + ROPE)
    query_rope = jnp.transpose(rotate(queries[:, :, NOPE:], block_pos), (1, 0, 2))
    head_first = tp_rank * heads_mla
    up_keys = lax.dynamic_slice_in_dim(key_up, head_first * NOPE, heads_mla * NOPE, 1)
    up_keys = up_keys.reshape(KV_RANK, heads_mla, NOPE)
    query_latent = jnp.einsum(
        "thn,jhn->htj", queries[:, :, :NOPE], up_keys, preferred_element_type=jnp.float32
    ).astype(jnp.bfloat16)
    mla_scale = (NOPE + ROPE) ** (-0.5)
    every_latent, every_rope = in_one_piece((query_latent, query_rope), "tp", 0, 2)
    slice_latent, slice_rope = (
        gather_axes(keys_latent, SP, (0, 1), 0),
        gather_axes(keys_rope, SP, (0, 1), 0),
    )
    heads_all = every_latent.shape[0]
    row_index = jnp.arange(slice_latent.shape[0], dtype=jnp.int32)
    slice_pos = row_index // own_rows * block_rows + tp_rank * own_rows + row_index % own_rows
    slice_state = (
        jnp.full((heads_all, block_rows), MASKED_VALUE, jnp.float32),
        jnp.zeros((heads_all, block_rows), jnp.float32),
        jnp.zeros((heads_all, block_rows, KV_RANK), jnp.float32),
    )
    part_max, part_sum, part_weighted = attend_latent(
        slice_state,
        slice_latent,
        slice_rope,
        slice_pos,
        every_latent,
        every_rope,
        block_pos,
        mla_scale,
    )
    global_max = of_everyone(part_max, "tp")
    rescale = jnp.exp(part_max - global_max)
    denom_sum, weighted = tuple(
        (
            part.astype(jnp.float32)
            for part in in_one_piece_2(
                (
                    (part_sum * rescale).astype(jnp.bfloat16),
                    (part_weighted * rescale[..., None]).astype(jnp.bfloat16),
                ),
                "tp",
                0,
                2,
            )
        )
    )
    latent_out = (weighted / denom_sum[..., None]).astype(jnp.bfloat16)
    up_values = lax.dynamic_slice_in_dim(value_up, head_first * VDIM, heads_mla * VDIM, 1)
    up_values = up_values.reshape(KV_RANK, heads_mla, VDIM)
    mla_out = jnp.einsum(
        "htj,jhv->thv", latent_out, up_values, preferred_element_type=jnp.float32
    ).astype(jnp.bfloat16)
    mla_out = mla_out.reshape(block_rows, heads_mla * VDIM)
    swa_q = projected[:, width_mla : width_mla + width_swa].reshape(
        block_rows, groups_kv, group, HEAD
    )
    swa_k = projected[:, width_mla + width_swa : width_mla + width_swa + width_kv]
    swa_v = projected[:, width_mla + width_swa + width_kv : width_mla + width_swa + 2 * width_kv]
    prev_keys, prev_values = from_behind(
        (swa_k[block_rows - WINDOW :], swa_v[block_rows - WINDOW :]), SP, 1
    )
    window_keys_all = jnp.concatenate([prev_keys, swa_k], axis=0).reshape(
        WINDOW + block_rows, groups_kv, HEAD
    )
    window_values = jnp.concatenate([prev_values, swa_v], axis=0).reshape(
        WINDOW + block_rows, groups_kv, HEAD
    )
    scores = jnp.einsum(
        "tkgd,skd->kgts", swa_q, window_keys_all, preferred_element_type=jnp.float32
    ) * HEAD ** (-0.5)
    key_pos = offset - WINDOW + jnp.arange(WINDOW + block_rows, dtype=jnp.int32)
    distance = block_pos[:, None] - key_pos[None, :]
    allowed = (distance >= 0) & (distance < WINDOW) & (key_pos[None, :] >= 0)
    scores = jnp.where(allowed, scores, MASKED_VALUE)
    sink_table = lax.dynamic_slice_in_dim(sink_logits, tp_rank * heads_swa, heads_swa, 0)
    sink_table = sink_table.reshape(groups_kv, group, 1, 1)
    row_max = jnp.maximum(jnp.max(scores, axis=-1, keepdims=True), sink_table)
    weights_raw = jnp.exp(scores - row_max)
    weights = (
        weights_raw / (jnp.sum(weights_raw, axis=-1, keepdims=True) + jnp.exp(sink_table - row_max))
    ).astype(jnp.bfloat16)
    swa_out = jnp.einsum(
        "kgts,skd->tkgd", weights, window_values, preferred_element_type=jnp.float32
    ).astype(jnp.bfloat16)
    swa_out = swa_out.reshape(block_rows, heads_swa * HEAD)
    all_mla, all_swa = in_one_piece((mla_out, swa_out), "tp", 1, 0)
    mixed = jnp.dot(all_mla, out_mla, preferred_element_type=jnp.float32) + jnp.dot(
        all_swa, out_swa, preferred_element_type=jnp.float32
    )
    return mixed.astype(jnp.bfloat16)


def solution(mesh):
    split = Mesh(mesh.devices.reshape(8, 8, mesh.shape["tp"]), ("sp_0", "sp_1", "tp"))
    placed = (
        P(SP_TP, None),
        P(),
        P(SP, None),
        P(SP, None),
        P(),
        P(None, "tp"),
        P(),
        P(),
        P(None, "tp"),
        P(None, "tp"),
        P(None, "tp"),
        P(),
        P(None, "tp"),
        P(None, "tp"),
    )
    return jax.shard_map(
        shards, mesh=split, in_specs=placed, out_specs=P(SP, "tp"), check_vma=False
    )
```

profile of v0, /device:TPU:1, one launch (start us, length us, event | category | flops | bytes accessed | tf_op | source)
XLA Modules:
  0.0 359.5 jit_solution(10568069677121225495)
XLA Ops:
  6.5 1.4 pad_maximum_fusion.3
  10.1 1.4 broadcast_in_dim.68
  11.5 10.3 %all-to-all-start = ((bf16[8,48,2048]{2,1,0:T(8,128)(2,1)}), bf16[8,48,2048]{2,1,0:T(8,128)(2,1)S(1)}, u32[]{:S(2)}, u32[]{:S(2)}) async-start(bf16[8,48,2048]{2,1,0:T(8,128)(2,1)} %broadcast_in_dim.68), calls=%async_computation | async-start | bytes 3145728 | tf_op jit(solution)/shard_map/all_to_all | solution.py:30
  21.8 20.6 %all-to-all-done = bf16[8,48,2048]{2,1,0:T(8,128)(2,1)S(1)} async-done(((bf16[8,48,2048]{2,1,0:T(8,128)(2,1)}), bf16[8,48,2048]{2,1,0:T(8,128)(2,1)S(1)}, u32[]{:S(2)}, u32[]{:S(2)}) %all-to-all-start) | async-done | bytes 1572896 | tf_op jit(solution)/shard_map/all_to_all | solution.py:30
  45.3 48.9 %all-gather.6.cloned.1.call-done = bf16[2048,320]{1,0:T(8,128)(2,1)} async-done(((bf16[32,320]{1,0:T(8,128)(2,1)}), bf16[2048,320]{1,0:T(8,128)(2,1)}) %all-gather.6.cloned.1.call-update) | async-done | bytes 1310736 | tf_op jit(solution)/shard_map/all_gather | solution.py:43
  94.2 1.5 convolution_convert_fusion.7
  95.9 20.3 %all-gather = bf16[384,256]{1,0:T(8,128)(2,1)} all-gather(bf16[48,256]{1,0:T(8,128)(2,1)S(1)} %fusion.52), channel_id=2, replica_groups=mesh['sp_0'=8,'sp_1'=8,'tp'=8] {'sp_0'}, dimensions={0}, use_global_device_ids=true | all-gather | bytes 221184 | tf_op jit(solution)/shard_map/all_gather | solution.py:49
  117.0 1.3 convolution_convert_fusion.8
  118.6 18.9 %all_gather.25 = bf16[8,48,64]{2,1,0:T(8,128)(2,1)S(1)} all-gather(bf16[1,48,64]{2,1,0:T(8,128)(2,1)S(1)} %pad_maximum_fusion.4), channel_id=1, replica_groups=mesh['sp_0'=8,'sp_1'=8,'tp'=8] {'sp_0'}, dimensions={0}, use_global_device_ids=true | all-gather | bytes 55296 | tf_op jit(solution)/shard_map/all_gather | solution.py:49
  137.5 23.1 %all_gather.26 = bf16[64,48,64]{2,1,0:T(8,128)(2,1)S(1)} all-gather(bf16[8,48,64]{2,1,0:T(8,128)(2,1)S(1)} %all_gather.25), channel_id=1, replica_groups=mesh['sp_0'=8,'sp_1'=8,'tp'=8] {'sp_1'}, dimensions={0}, use_global_device_ids=true | all-gather | bytes 442368 | tf_op jit(solution)/shard_map/all_gather | solution.py:49
  160.5 1.6 copy.34
  162.2 2.0 reshape_reshape.7
  164.2 2.7 split.33
  166.9 1.7 copy.35
  169.7 2.7 copy.33
  172.5 1.9 broadcast_in_dim.66
  174.4 22.4 %while.18 = (s32[]{:T(128)}, f32[8,384]{1,0:T(8,128)S(1)}, f32[8,384]{1,0:T(8,128)S(1)}, f32[8,384,256]{2,1,0:T(8,128)}, s32[3072]{0:T(1024)S(1)}, /*index=5*/s3...) while((s32[]{:T(128)}, f32[8,384]{1,0:T(8,128)S(1)}, ...), condition=%wide.region_7.8_spmd.clone, body=%wide.region_2.7_spmd.clone.sunk | while | flops 1829443968 | bytes 66466276 | solution.py:151
  176.4 10.4 %conditional.3 = ((f32[8,384]{1,0:T(8,128)S(1)}, f32[8,384]{1,0:T(8,128)S(1)}, f32[8,384,256]{2,1,0:T(8,128)})) conditional(s32[]{:T(128)} %convert_element_type.210, (f32[8,384]{1,0:T(8,128)S(1)}, f32[8,384]{1,0:T(8,128)S(1)}, f32[8,384,256]{2,1,0:T(8,128)}) %tuple.52, (s32[512]{0:T(512)S(1)}, s32[]{:T(128)}, s32[]{:T(128)}, ...), branch_computations={%region_3.3_spmd, %region_4.6_spmd} | conditional | flops 1829443968 | bytes 66460312 | solution.py:149
  177.6 2.5 fusion.85
  180.2 1.1 fusion.3
  182.0 3.1 multiply_add_fusion
  185.1 1.6 copy-done.2
  196.8 29.9 %all_to_all.10 = f32[8,8,384]{2,1,0:T(8,128)S(1)} all-to-all(f32[8,8,384]{2,1,0:T(8,128)S(1)} %broadcast_in_dim.69), channel_id=1, replica_groups=mesh['sp_0'=8,'sp_1'=8,'tp'=8] {'tp'}, dimensions={0} | all-to-all | bytes 196608 | tf_op jit(solution)/shard_map/all_to_all | solution.py:30
  227.2 2.4 multiply_convert_fusion
  229.5 2.5 pad_maximum_fusion
  234.1 2.6 collective-permute-start.1
  237.4 3.1 collective-permute-start
  242.4 73.9 %reduce-scatter.2.cloned.1.call-done = bf16[1,384,257]{2,1,0:T(8,128)(2,1)} async-done(((bf16[8,384,257]{2,1,0:T(8,128)(2,1)}), bf16[1,384,257]{2,1,0:T(8,128)(2,1)}) %reduce-scatter.2.cloned.1.call-update) | async-done | bytes 197392 | tf_op jit(solution)/shard_map/reduce_scatter | solution.py:70
  317.3 1.3 fusion.26
  319.3 30.9 %all-gather.12.cloned.1.call-done = bf16[768,1024]{0,1:T(8,128)(2,1)} async-done(((bf16[768,128]{0,1:T(8,128)(2,1)}), bf16[768,1024]{0,1:T(8,128)(2,1)}) %all-gather.12.cloned.1.call-update) | async-done | bytes 1572880 | tf_op jit(solution)/shard_map/all_gather | solution.py:43
  350.2 1.7 fusion.29
  351.9 1.1 fusion.23
  (112 shorter events, 19.6 us)
Async XLA Ops:
  6.5 35.9 %copy-start = (bf16[2048,192]{0,1:T(8,128)(2,1)S(1)}, bf16[2048,192]{0,1:T(8,128)(2,1)}, u32[]{:S(2)}) copy-start(bf16[2048,192]{0,1:T(8,128)(2,1)} %param.23) | copy-start | bytes 2359300
  6.5 87.7 %all-gather.6.cloned.1.call-start = ((), (), s32[]{:S(2)}) async-start(), calls=%async_computation.3 | async-start | bytes 1597440 | tf_op jit(solution)/shard_map/all_gather | solution.py:43
  11.5 30.9 %all-to-all-start = ((bf16[8,48,2048]{2,1,0:T(8,128)(2,1)}), bf16[8,48,2048]{2,1,0:T(8,128)(2,1)S(1)}, u32[]{:S(2)}, u32[]{:S(2)}) async-start(bf16[8,48,2048]{2,1,0:T(8,128)(2,1)} %broadcast_in_dim.68), calls=%async_computation | async-start | bytes 3145728 | tf_op jit(solution)/shard_map/all_to_all | solution.py:30
  21.8 142.4 %all-gather.10.cloned.1.call-start = ((), (), s32[]{:S(2)}) async-start(), calls=%async_computation.5 | async-start | bytes 2211840 | tf_op jit(solution)/shard_map/all_gather | solution.py:43
  42.4 1.8 copy-start.3
  43.1 52.7 %copy-start.8 = (f32[256]{0:T(256)S(1)}, f32[256]{0:T(256)}, u32[]{:S(2)}) copy-start(f32[256]{0:T(256)} %param.22) | copy-start | bytes 3076
  45.2 124.5 %all-gather.8.cloned.1.call-start = ((), (), s32[]{:S(2)}) async-start(), calls=%async_computation.4 | async-start | bytes 1769472 | tf_op jit(solution)/shard_map/all_gather | solution.py:49
  116.3 200.0 %reduce-scatter.2.cloned.1.call-start = ((), (), s32[]{:S(2)}) async-start(), calls=%async_computation.6 | async-start | bytes 2654208 | tf_op jit(solution)/shard_map/reduce_scatter | solution.py:70
  180.1 1.9 copy-start.1
  185.1 1.6 copy-start.2
  232.0 0.7 copy-start.12
  232.0 1.4 copy-start.4
  232.0 1.4 copy-start.6
  232.1 4.7 %copy-start.7 = (bf16[2048,64]{0,1:T(8,128)(2,1)S(1)}, bf16[2048,64]{0,1:T(8,128)(2,1)}, u32[]{:S(2)}) copy-start(bf16[2048,64]{0,1:T(8,128)(2,1)} %param.28) | copy-start | bytes 786436
  232.1 118.1 %all-gather.12.cloned.1.call-start = ((), (), s32[]{:S(2)}) async-start(), calls=%async_computation.7 | async-start | bytes 1769472 | tf_op jit(solution)/shard_map/all_gather | solution.py:43
  233.5 7.0 %copy-start.5 = (bf16[2048,128]{1,0:T(8,128)(2,1)S(1)}, bf16[2048,128]{1,0:T(8,128)(2,1)}, u32[]{:S(2)}) copy-start(bf16[2048,128]{1,0:T(8,128)(2,1)} %param.26) | copy-start | bytes 1572868
  234.1 7.0 %collective-permute-start.1 = (bf16[128,64]{0,1:T(8,128)(2,1)S(1)}, bf16[128,64]{0,1:T(8,128)(2,1)S(1)}, u32[]{:S(2)}, u32[]{:S(2)}) collective-permute-start(bf16[128,64]{0,1:T(8,128)(2,1)S(1)} %slice.51), channel_id=1, source_target_pairs={{0,8},{8,16},{16,24},{24,32},{32,40},{40,48},{48,56},{56,64},{64,7... | collective-permute-start | bytes 49160 | tf_op jit(solution)/shard_map/ppermute | solution.py:80
  237.4 4.6 %collective-permute-start = (bf16[128,64]{0,1:T(8,128)(2,1)S(1)}, bf16[128,64]{0,1:T(8,128)(2,1)S(1)}, u32[]{:S(2)}, u32[]{:S(2)}) collective-permute-start(bf16[128,64]{0,1:T(8,128)(2,1)S(1)} %slice.50), channel_id=1, source_target_pairs={{0,8},{8,16},{16,24},{24,32},{32,40},{40,48},{48,56},{56,64},{64,7... | collective-permute-start | bytes 49160 | tf_op jit(solution)/shard_map/ppermute | solution.py:80
  242.4 107.8 %copy-start.10 = (bf16[1024,256]{1,0:T(8,128)(2,1)S(1)}, bf16[1024,256]{1,0:T(8,128)(2,1)}, u32[]{:S(2)}) copy-start(bf16[1024,256]{1,0:T(8,128)(2,1)} %param.30) | copy-start | bytes 1572868
  318.6 33.3 %copy-start.11 = (bf16[1024,256]{1,0:T(8,128)(2,1)S(1)}, bf16[1024,256]{1,0:T(8,128)(2,1)}, u32[]{:S(2)}) copy-start(bf16[1024,256]{1,0:T(8,128)(2,1)} %param.31) | copy-start | bytes 1572868
  350.2 1.7 copy-start.9
Sparse Core Ops, SparseCore 0:
  10.3 83.8 all-gather.5
  96.3 32.2 all-gather.9
  130.7 38.5 all-gather.7
  232.2 84.0 reduce-scatter.1
  319.5 30.6 all-gather.11
where the time goes:
time: 361 us; the launch traced here: 360 us
  waiting for transfers between devices  174 us (48%)
  blocking collectives  92.2 us (26%)
  local copies, waits for them, and re-layouts  23.2 us (6%)
  matrix products  17.9 us (5%)
  starting transfers between devices  16.4 us (5%)
  other arithmetic  13.6 us (4%)
  between operations  13.5 us (4%)
  loops' own time  8.35 us (2%)
    all_gather x3, waiting for transfers between devices, in_one_piece(): lax.all_gather(both, axis, axis=dim, tiled=True)  79.8 us
    reduce_scatter x1, waiting for transfers between devices, in_one_piece_2(): result = lax.psum_scatter(both, axis, scatter_dimension=dim, tiled=True)  73.9 us
    all_gather x3, blocking collectives, stacked_from(): tiles = lax.all_gather(tiles, axes[k], axis=0, tiled=True)  62.3 us
    all_to_all x1, blocking collectives, copy_for_each(): return lax.all_to_all(copies, axis, split_axis=0, concat_axis=0, tiled=True)  29.9 us
    all_to_all x1, waiting for transfers between devices, copy_for_each(): return lax.all_to_all(copies, axis, split_axis=0, concat_axis=0, tiled=True)  20.6 us
    all_to_all x1, starting transfers between devices, copy_for_each(): return lax.all_to_all(copies, axis, split_axis=0, concat_axis=0, tiled=True)  10.3 us
    another operation x1, loops' own time, attend_latent(): return lax.fori_loop(0, key_count // span_rows, update, state_in)  8.16 us
  transfers between devices with their start and end apart: 8, of which 4 were waited for; matrix products, arithmetic and copies ran while one was open for 6% of the time, Pallas kernels for 0%

commit v1 on v0

--- a/solution.py
+++ b/solution.py
@@ -46,7 +46,9 @@
 def stacked_from(array, axes, turns):
     tiles = array[None]
     for k in turns:
-        tiles = lax.all_gather(tiles, axes[k], axis=0, tiled=True)
+        tiles = jnp.concatenate(
+            lax.all_to_all(jnp.stack([tiles] * lax.axis_size(axes[k])), axes[k], 0, 0), axis=0
+        )
     held = [lax.axis_size(axes[k]) for k in reversed(turns)]
     tiles = tiles.reshape(*held, *array.shape)
     turned = sorted(range(len(turns)), key=lambda place: turns[len(turns) - 1 - place])

time: 361 us -> 351 us (0.972)
  blocking collectives: 92.2 us -> 31.4 us
  waiting for transfers between devices: 174 us -> 208 us
  starting transfers between devices: 16.4 us -> 27.2 us
  local copies, waits for them, and re-layouts: 23.2 us -> 27.4 us
    all_gather x3 -> x0, blocking collectives: 62.3 us -> none  [stacked_from(): tiles = lax.all_gather(tiles, axes[k], axis=0, tiled=True)]
    all_to_all x0 -> x3, waiting for transfers between devices: none -> 32.4 us  [stacked_from(): lax.all_to_all(jnp.stack([tiles] * lax.axis_size(axes[k])), axes[k], 0, 0)]
    all_to_all x0 -> x1, blocking collectives: none -> 15.1 us  [stacked_from(): lax.all_to_all(jnp.stack([tiles] * lax.axis_size(axes[k])), axes[k], 0, 0)]
    all_to_all x1, blocking collectives: 29.9 us -> 16.3 us  [copy_for_each(): return lax.all_to_all(copies, axis, split_axis=0, concat_axis=0, tiled=True)]
    all_to_all x0 -> x3, starting transfers between devices: none -> 12 us  [stacked_from(): lax.all_to_all(jnp.stack([tiles] * lax.axis_size(axes[k])), axes[k], 0, 0)]
    all_gather x3, waiting for transfers between devices: 79.8 us -> 85.1 us  [in_one_piece(): lax.all_gather(both, axis, axis=dim, tiled=True)]
    reduce_scatter x1, waiting for transfers between devices: 73.9 us -> 69.9 us  [in_one_piece_2(): result = lax.psum_scatter(both, axis, scatter_dimension=dim, tiled=True)]
  transfers between devices with their start and end apart: 8 -> 10, of which waited for: 4 -> 8; matrix products, arithmetic and copies ran while one was open for 6% -> 6% of each run, Pallas kernels for 0% -> 0%
where the time goes in v1:
time: 351 us; the launch traced here: 350 us
  waiting for transfers between devices  208 us (59%)
  blocking collectives  31.4 us (9%)
  local copies, waits for them, and re-layouts  27.4 us (8%)
  starting transfers between devices  27.2 us (8%)
  matrix products  18.9 us (5%)
  between operations  15.4 us (4%)
  other arithmetic  13.5 us (4%)
  loops' own time  7.9 us (2%)
    all_gather x3, waiting for transfers between devices, in_one_piece(): lax.all_gather(both, axis, axis=dim, tiled=True)  85.1 us
    reduce_scatter x1, waiting for transfers between devices, in_one_piece_2(): result = lax.psum_scatter(both, axis, scatter_dimension=dim, tiled=True)  69.9 us
    all_to_all x3, waiting for transfers between devices, stacked_from(): lax.all_to_all(jnp.stack([tiles] * lax.axis_size(axes[k])), axes[k], 0, 0)  32.4 us
    all_to_all x1, waiting for transfers between devices, copy_for_each(): return lax.all_to_all(copies, axis, split_axis=0, concat_axis=0, tiled=True)  20.6 us
    all_to_all x1, blocking collectives, copy_for_each(): return lax.all_to_all(copies, axis, split_axis=0, concat_axis=0, tiled=True)  16.3 us
    all_to_all x1, blocking collectives, stacked_from(): lax.all_to_all(jnp.stack([tiles] * lax.axis_size(axes[k])), axes[k], 0, 0)  15.1 us
    all_to_all x3, starting transfers between devices, stacked_from(): lax.all_to_all(jnp.stack([tiles] * lax.axis_size(axes[k])), axes[k], 0, 0)  12 us
    all_to_all x1, starting transfers between devices, copy_for_each(): return lax.all_to_all(copies, axis, split_axis=0, concat_axis=0, tiled=True)  10.3 us
  transfers between devices with their start and end apart: 10, of which 8 were waited for; matrix products, arithmetic and copies ran while one was open for 6% of the time, Pallas kernels for 0%

profile of v1, /device:TPU:1, one launch (start us, length us, event | category | flops | bytes accessed | tf_op | source)
XLA Modules:
  0.0 349.6 jit_solution(5283499771203252947)
XLA Ops:
  12.3 10.3 %all-to-all-start.2 = ((bf16[8,48,2048]{2,1,0:T(8,128)(2,1)}), bf16[8,48,2048]{2,1,0:T(8,128)(2,1)S(1)}, u32[]{:S(2)}, u32[]{:S(2)}) async-start(bf16[8,48,2048]{2,1,0:T(8,128)(2,1)} %broadcast_in_dim.63), calls=%async_computation.2 | async-start | bytes 3145728 | tf_op jit(solution)/shard_map/all_to_all | solution.py:30
  22.7 20.6 %all-to-all-done.2 = bf16[8,48,2048]{2,1,0:T(8,128)(2,1)S(1)} async-done(((bf16[8,48,2048]{2,1,0:T(8,128)(2,1)}), bf16[8,48,2048]{2,1,0:T(8,128)(2,1)S(1)}, u32[]{:S(2)}, u32[]{:S(2)}) %all-to-all-start.2) | async-done | bytes 1572896 | tf_op jit(solution)/shard_map/all_to_all | solution.py:30
  45.0 50.0 %all-gather.4.cloned.1.call-done = bf16[2048,320]{1,0:T(8,128)(2,1)} async-done(((bf16[32,320]{1,0:T(8,128)(2,1)}), bf16[2048,320]{1,0:T(8,128)(2,1)}) %all-gather.4.cloned.1.call-update) | async-done | bytes 1310736 | tf_op jit(solution)/shard_map/all_gather | solution.py:43
  95.0 1.5 convolution_convert_fusion.7
  99.0 4.3 %all-to-all-start.3 = ((bf16[8,2,1536]{2,1,0:T(2,128)(2,1)}), bf16[8,2,1536]{2,1,0:T(2,128)(2,1)S(1)}, u32[]{:S(2)}, u32[]{:S(2)}) async-start(bf16[8,2,1536]{2,1,0:T(2,128)(2,1)} %reshape.368), calls=%async_computation.3 | async-start | bytes 98304 | tf_op jit(solution)/shard_map/all_to_all | solution.py:50
  103.4 7.0 %all-to-all-done.3 = bf16[8,2,1536]{2,1,0:T(2,128)(2,1)S(1)} async-done(((bf16[8,2,1536]{2,1,0:T(2,128)(2,1)}), bf16[8,2,1536]{2,1,0:T(2,128)(2,1)S(1)}, u32[]{:S(2)}, u32[]{:S(2)}) %all-to-all-start.3) | async-done | bytes 49184 | tf_op jit(solution)/shard_map/all_to_all | solution.py:50
  111.0 3.4 all-to-all-start
  116.3 6.7 %all-to-all-done = bf16[8,1,48,256]{3,2,1,0:T(8,128)(2,1)S(1)} async-done(((bf16[8,1,48,256]{3,2,1,0:T(8,128)(2,1)}), bf16[8,1,48,256]{3,2,1,0:T(8,128)(2,1)S(1)}, u32[]{:S(2)}, u32[]{:S(2)}) %all-to-all-start) | async-done | bytes 196640 | tf_op jit(solution)/shard_map/all_to_all | solution.py:50
  123.0 15.1 %all_to_all.30 = bf16[8,2,12288]{2,1,0:T(2,128)(2,1)S(1)} all-to-all(bf16[8,2,12288]{2,1,0:T(2,128)(2,1)S(1)} %reshape.370), channel_id=1, replica_groups=mesh['sp_0'=8,'sp_1'=8,'tp'=8] {'sp_1'}, dimensions={0} | all-to-all | bytes 786432 | tf_op jit(solution)/shard_map/all_to_all | solution.py:50
  139.4 4.3 %all-to-all-start.1 = ((bf16[8,8,48,256]{3,2,1,0:T(8,128)(2,1)}), bf16[8,8,48,256]{3,2,1,0:T(8,128)(2,1)}, u32[]{:S(2)}, u32[]{:S(2)}) async-start(bf16[8,8,48,256]{3,2,1,0:T(8,128)(2,1)} %stack.13), calls=%async_computation.1 | async-start | bytes 3145728 | tf_op jit(solution)/shard_map/all_to_all | solution.py:50
  145.1 1.7 copy.37
  146.7 2.0 reshape_reshape.7
  148.8 4.4 %all-gather.6.cloned.1.call-done = bf16[8,384,320]{1,2,0:T(8,128)(2,1)} async-done(((bf16[1,384,320]{1,2,0:T(8,128)(2,1)}), bf16[8,384,320]{1,2,0:T(8,128)(2,1)}) %all-gather.6.cloned.1.call-update) | async-done | bytes 1966096 | tf_op jit(solution)/shard_map/all_gather | solution.py:43
  153.1 2.7 split.33
  155.9 1.7 copy.38
  158.6 18.7 %all-to-all-done.1 = bf16[8,8,48,256]{3,2,1,0:T(8,128)(2,1)} async-done(((bf16[8,8,48,256]{3,2,1,0:T(8,128)(2,1)}), bf16[8,8,48,256]{3,2,1,0:T(8,128)(2,1)}, u32[]{:S(2)}, u32[]{:S(2)}) %all-to-all-start.1) | async-done | bytes 1572896 | tf_op jit(solution)/shard_map/all_to_all | solution.py:50
  177.4 2.8 copy.36
  180.1 1.9 broadcast_in_dim.62
  182.0 22.0 %while.18 = (s32[]{:T(128)}, f32[8,384]{1,0:T(8,128)S(1)}, f32[8,384]{1,0:T(8,128)S(1)}, f32[8,384,256]{2,1,0:T(8,128)}, s32[3072]{0:T(1024)S(1)}, /*index=5*/s3...) while((s32[]{:T(128)}, f32[8,384]{1,0:T(8,128)S(1)}, ...), condition=%wide.region_7.8_spmd.clone, body=%wide.region_2.7_spmd.clone.sunk | while | flops 1829443968 | bytes 66466276 | solution.py:153
  183.9 10.4 %conditional.3 = ((f32[8,384]{1,0:T(8,128)S(1)}, f32[8,384]{1,0:T(8,128)S(1)}, f32[8,384,256]{2,1,0:T(8,128)})) conditional(s32[]{:T(128)} %convert_element_type.208, (f32[8,384]{1,0:T(8,128)S(1)}, f32[8,384]{1,0:T(8,128)S(1)}, f32[8,384,256]{2,1,0:T(8,128)}) %tuple.53, (s32[512]{0:T(512)S(1)}, s32[]{:T(128)}, s32[]{:T(128)}, ...), branch_computations={%region_3.3_spmd, %region_4.6_spmd} | conditional | flops 1829443968 | bytes 66460312 | solution.py:151
  185.1 2.5 fusion.83
  189.6 3.1 multiply_add_fusion
  192.7 1.6 copy-done.2
  204.1 16.3 %all_to_all.31 = f32[8,8,384]{2,1,0:T(8,128)S(1)} all-to-all(f32[8,8,384]{2,1,0:T(8,128)S(1)} %broadcast_in_dim.64), channel_id=1, replica_groups=mesh['sp_0'=8,'sp_1'=8,'tp'=8] {'tp'}, dimensions={0} | all-to-all | bytes 196608 | tf_op jit(solution)/shard_map/all_to_all | solution.py:30
  220.8 2.4 multiply_convert_fusion
  223.2 2.5 pad_maximum_fusion
  227.7 1.8 collective-permute-start.1
  230.2 2.5 collective-permute-start
  234.5 69.9 %reduce-scatter.2.cloned.1.call-done = bf16[1,384,257]{2,1,0:T(8,128)(2,1)} async-done(((bf16[8,384,257]{2,1,0:T(8,128)(2,1)}), bf16[1,384,257]{2,1,0:T(8,128)(2,1)}) %reduce-scatter.2.cloned.1.call-update) | async-done | bytes 197392 | tf_op jit(solution)/shard_map/reduce_scatter | solution.py:72
  307.5 30.7 %all-gather.8.cloned.1.call-done = bf16[768,1024]{0,1:T(8,128)(2,1)} async-done(((bf16[768,128]{0,1:T(8,128)(2,1)}), bf16[768,1024]{0,1:T(8,128)(2,1)}) %all-gather.8.cloned.1.call-update) | async-done | bytes 1572880 | tf_op jit(solution)/shard_map/all_gather | solution.py:43
  338.2 1.7 fusion.29
  339.9 2.1 fusion.23
  (119 shorter events, 30.3 us)
Async XLA Ops:
  7.4 35.9 %copy-start = (bf16[2048,192]{0,1:T(8,128)(2,1)S(1)}, bf16[2048,192]{0,1:T(8,128)(2,1)}, u32[]{:S(2)}) copy-start(bf16[2048,192]{0,1:T(8,128)(2,1)} %param.23) | copy-start | bytes 2359300
  7.4 87.7 %all-gather.4.cloned.1.call-start = ((), (), s32[]{:S(2)}) async-start(), calls=%async_computation.7 | async-start | bytes 1597440 | tf_op jit(solution)/shard_map/all_gather | solution.py:43
  12.3 30.9 %all-to-all-start.2 = ((bf16[8,48,2048]{2,1,0:T(8,128)(2,1)}), bf16[8,48,2048]{2,1,0:T(8,128)(2,1)S(1)}, u32[]{:S(2)}, u32[]{:S(2)}) async-start(bf16[8,48,2048]{2,1,0:T(8,128)(2,1)} %broadcast_in_dim.63), calls=%async_computation.2 | async-start | bytes 3145728 | tf_op jit(solution)/shard_map/all_to_all | solution.py:30
  43.3 1.8 copy-start.3
  43.9 59.4 %copy-start.8 = (f32[256]{0:T(256)S(1)}, f32[256]{0:T(256)}, u32[]{:S(2)}) copy-start(f32[256]{0:T(256)} %param.22) | copy-start | bytes 3076
  99.0 11.4 %all-to-all-start.3 = ((bf16[8,2,1536]{2,1,0:T(2,128)(2,1)}), bf16[8,2,1536]{2,1,0:T(2,128)(2,1)S(1)}, u32[]{:S(2)}, u32[]{:S(2)}) async-start(bf16[8,2,1536]{2,1,0:T(2,128)(2,1)} %reshape.368), calls=%async_computation.3 | async-start | bytes 98304 | tf_op jit(solution)/shard_map/all_to_all | solution.py:50
  111.0 11.9 %all-to-all-start = ((bf16[8,1,48,256]{3,2,1,0:T(8,128)(2,1)}), bf16[8,1,48,256]{3,2,1,0:T(8,128)(2,1)S(1)}, u32[]{:S(2)}, u32[]{:S(2)}) async-start(bf16[8,1,48,256]{3,2,1,0:T(8,128)(2,1)} %stack.12), calls=%async_computation | async-start | bytes 393216 | tf_op jit(solution)/shard_map/all_to_all | solution.py:50
  114.4 38.7 %all-gather.6.cloned.1.call-start = ((), (), s32[]{:S(2)}) async-start(), calls=%async_computation.8 | async-start | bytes 2211840 | tf_op jit(solution)/shard_map/all_gather | solution.py:43
  139.4 38.0 %all-to-all-start.1 = ((bf16[8,8,48,256]{3,2,1,0:T(8,128)(2,1)}), bf16[8,8,48,256]{3,2,1,0:T(8,128)(2,1)}, u32[]{:S(2)}, u32[]{:S(2)}) async-start(bf16[8,8,48,256]{3,2,1,0:T(8,128)(2,1)} %stack.13), calls=%async_computation.1 | async-start | bytes 3145728 | tf_op jit(solution)/shard_map/all_to_all | solution.py:50
  143.7 160.7 %reduce-scatter.2.cloned.1.call-start = ((), (), s32[]{:S(2)}) async-start(), calls=%async_computation.9 | async-start | bytes 2654208 | tf_op jit(solution)/shard_map/reduce_scatter | solution.py:72
  187.7 1.9 copy-start.1
  192.7 1.7 copy-start.2
  225.7 0.7 copy-start.11
  225.7 1.4 copy-start.4
  225.7 1.4 copy-start.6
  225.7 3.9 %copy-start.7 = (bf16[2048,64]{0,1:T(8,128)(2,1)S(1)}, bf16[2048,64]{0,1:T(8,128)(2,1)}, u32[]{:S(2)}) copy-start(bf16[2048,64]{0,1:T(8,128)(2,1)} %param.28) | copy-start | bytes 786436
  225.7 112.5 %all-gather.8.cloned.1.call-start = ((), (), s32[]{:S(2)}) async-start(), calls=%async_computation.10 | async-start | bytes 1769472 | tf_op jit(solution)/shard_map/all_gather | solution.py:43
  227.1 5.5 %copy-start.5 = (bf16[2048,128]{1,0:T(8,128)(2,1)S(1)}, bf16[2048,128]{1,0:T(8,128)(2,1)}, u32[]{:S(2)}) copy-start(bf16[2048,128]{1,0:T(8,128)(2,1)} %param.26) | copy-start | bytes 1572868
  227.7 5.5 %collective-permute-start.1 = (bf16[128,64]{0,1:T(8,128)(2,1)S(1)}, bf16[128,64]{0,1:T(8,128)(2,1)S(1)}, u32[]{:S(2)}, u32[]{:S(2)}) collective-permute-start(bf16[128,64]{0,1:T(8,128)(2,1)S(1)} %slice.51), channel_id=1, source_target_pairs={{0,8},{8,16},{16,24},{24,32},{32,40},{40,48},{48,56},{56,64},{64,7... | collective-permute-start | bytes 49160 | tf_op jit(solution)/shard_map/ppermute | solution.py:82
  230.2 3.9 %collective-permute-start = (bf16[128,64]{0,1:T(8,128)(2,1)S(1)}, bf16[128,64]{0,1:T(8,128)(2,1)S(1)}, u32[]{:S(2)}, u32[]{:S(2)}) collective-permute-start(bf16[128,64]{0,1:T(8,128)(2,1)S(1)} %slice.50), channel_id=1, source_target_pairs={{0,8},{8,16},{16,24},{24,32},{32,40},{40,48},{48,56},{56,64},{64,7... | collective-permute-start | bytes 49160 | tf_op jit(solution)/shard_map/ppermute | solution.py:82
  234.5 103.7 %copy-start.10 = (bf16[1024,256]{1,0:T(8,128)(2,1)S(1)}, bf16[1024,256]{1,0:T(8,128)(2,1)}, u32[]{:S(2)}) copy-start(bf16[1024,256]{1,0:T(8,128)(2,1)} %param.30) | copy-start | bytes 1572868
  338.2 1.7 copy-start.9
Sparse Core Ops, SparseCore 0:
  11.2 83.8 all-gather.3
Sparse Core Ops, SparseCore 1:
  117.0 36.0 all-gather.5
  225.8 78.6 reduce-scatter.1
  307.6 30.5 all-gather.7
